TPU v7x, 32 devices: a whole 2x2x4 slice. The times are simulated.
32 devices in a mesh: grp: 2 (over x), ep: 16 (over z, y, core), tp: 1.
Axes of the slice: x: 2, y: 2, z: 4, core: 2. Of those that a mesh axis runs over, the one named last changes fastest.
Arguments:
- tokens: bfloat16 [2048, 2048], P(('grp', 'ep')), parts along dimension 0, may hold values from -6 to 6
- norm_gain: float32 [2048], replicated, may hold values from 0.1 to 1.9
- expert_gate: bfloat16 [16, 2048, 512], P('ep', None, 'tp'), may hold values from -0.125 to 0.125
- expert_up: bfloat16 [16, 2048, 512], P('ep', None, 'tp'), may hold values from -0.125 to 0.125
- expert_down: bfloat16 [16, 512, 2048], P('ep', 'tp'), may hold values from -0.25 to 0.25
- shared_gate: bfloat16 [2048, 512], P(None, 'tp'), may hold values from -0.125 to 0.125
- shared_up: bfloat16 [2048, 512], P(None, 'tp'), may hold values from -0.125 to 0.125
- shared_down: bfloat16 [512, 2048], P('tp'), may hold values from -0.25 to 0.25
- routes: int32 [2048, 8], P(('grp', 'ep')), parts along dimension 0, may hold values from 0 to 15, all different within a row; in each aligned block of 64 rows (0 to 63, 64 to 127, ...) at most 64 rows name the same one
- route_weights: float32 [2048, 8], P(('grp', 'ep')), parts along dimension 0, may hold values from 0.05 to 0.6
Outputs:
- mixed: bfloat16 [2048, 2048], P(('grp', 'ep'), 'tp'), parts along dimension 0
There are 2 independent parts, one for each index of `grp`. A program takes and returns all parts, laid end to end along the dimension named above; an argument that names none is the same for every part. Nothing has to cross between parts.
Inputs may be any that keep to these rules, and one draw needn't show every extreme that they name: `routes`: each row names 8 different experts. Within the rows of one index of ep no expert is named more than 64 times, a bound that some block reaches by the rows of some index of ep.
All inputs are finite; a program needn't handle non-finite values.
Results may differ from a plain program's by a relative error of at most 0.0085.
Values may be sent and summed in bfloat16 or wider, within the bound.
A program may use at most 64 MiB of HBM per device.

v0:
```python
import jax
import jax.numpy as jnp
from jax import lax
from jax.sharding import PartitionSpec as P


def rms_scaled(values, gain):
    wide = values.astype(jnp.float32)
    scaled = wide * lax.rsqrt(jnp.mean(wide * wide, axis=-1, keepdims=True) + 1e-06)
    return (scaled * gain).astype(jnp.bfloat16)


def swiglu_partial(row_block, w_gate, w_up, w_down):
    gate_proj = jnp.dot(row_block, w_gate, preferred_element_type=jnp.float32)
    up_proj = jnp.dot(row_block, w_up, preferred_element_type=jnp.float32)
    hidden = (jax.nn.silu(gate_proj) * up_proj).astype(jnp.bfloat16)
    partial_value = jnp.dot(hidden, w_down, preferred_element_type=jnp.float32)
    return lax.optimization_barrier(partial_value.astype(jnp.bfloat16)).astype(jnp.float32)


def per_device(
    tokens,
    norm_gain,
    expert_gate,
    expert_up,
    expert_down,
    shared_gate,
    shared_up,
    shared_down,
    routes,
    route_weights,
):
    tok_rows = tokens.shape[0]
    model_width = tokens.shape[1]
    top_count = routes.shape[1]
    experts = lax.axis_size("ep")
    half_width = model_width // lax.axis_size("tp")
    capacity = min(tok_rows, 2 * tok_rows * top_count // experts)
    normed = rms_scaled(tokens, norm_gain)
    shared_part = swiglu_partial(normed, shared_gate, shared_up, shared_down)
    all_normed = lax.all_gather(normed, "ep", axis=0, tiled=True)
    all_routes = lax.all_gather(routes, "ep", axis=0, tiled=True)
    all_weights = lax.all_gather(route_weights, "ep", axis=0, tiled=True)
    own_expert = lax.axis_index("ep")
    hit_table = all_routes == own_expert
    is_mine = jnp.sum(hit_table.astype(jnp.int32), axis=1).reshape(experts, tok_rows)
    weight_mine = jnp.sum(jnp.where(hit_table, all_weights, jnp.float32(0.0)), axis=1).reshape(
        experts, tok_rows
    )
    slot_rank = jnp.cumsum(is_mine, axis=1) - is_mine
    matches = (slot_rank[:, None, :] == jnp.arange(capacity, dtype=jnp.int32)[None, :, None]) & (
        is_mine[:, None, :] == 1
    )
    slot_token = jnp.sum(
        jnp.where(matches, jnp.arange(tok_rows, dtype=jnp.int32)[None, None, :], 0), axis=2
    )
    slot_live = jnp.any(matches, axis=2).reshape(-1)
    slot_weight = jnp.sum(
        jnp.where(matches, weight_mine[:, None, :], jnp.float32(0.0)), axis=2
    ).reshape(-1)
    global_row = (jnp.arange(experts, dtype=jnp.int32)[:, None] * tok_rows + slot_token).reshape(-1)
    taken = jnp.take(all_normed, global_row, axis=0)
    inbound = jnp.where(slot_live[:, None], taken, jnp.zeros_like(taken))
    expert_part = swiglu_partial(inbound, expert_gate[0], expert_up[0], expert_down[0])
    expert_sum, shared_sum = (
        lax.psum_scatter(
            expert_part.astype(jnp.bfloat16), "tp", scatter_dimension=1, tiled=True
        ).astype(jnp.float32),
        lax.psum_scatter(
            shared_part.astype(jnp.bfloat16), "tp", scatter_dimension=1, tiled=True
        ).astype(jnp.float32),
    )
    expert_out = expert_sum.astype(jnp.bfloat16)
    shared_out = shared_sum.astype(jnp.bfloat16)
    weighted_rows = expert_out.astype(jnp.float32) * slot_weight[:, None]
    terms = (
        jnp.zeros((experts * tok_rows, half_width), jnp.float32).at[global_row].add(weighted_rows)
    )
    routed = lax.psum_scatter(terms, "ep", scatter_dimension=0, tiled=True)
    return (routed + shared_out.astype(jnp.float32)).astype(jnp.bfloat16)


def solution(mesh):
    in_specs = (
        P(("grp", "ep"), None),
        P(),
        P("ep", None, "tp"),
        P("ep", None, "tp"),
        P("ep", "tp", None),
        P(None, "tp"),
        P(None, "tp"),
        P("tp", None),
        P(("grp", "ep"), None),
        P(("grp", "ep"), None),
    )
    out_specs = P(("grp", "ep"), "tp")
    return jax.shard_map(
        per_device, mesh=mesh, in_specs=in_specs, out_specs=out_specs, check_vma=False
    )
```

profile of v0, /device:TPU:0, one launch (start us, length us, event | category | flops | bytes accessed | tf_op | source)
XLA Modules:
  0.0 220.2 jit_solution(10762716393236686828)
XLA Ops:
  6.5 0.0 copy-start
  6.5 0.0 all-gather.4.cloned.1.call-start
  6.5 1.2 fusion.15
  7.8 1.8 fusion.17
  9.6 0.0 all-gather.4.cloned.1.call-update
  9.6 0.0 reduce-scatter.2.cloned.1.call-start
  9.7 23.8 %all-gather = s32[16,64,8]{1,2,0:T(8,128)S(1)} all-gather(s32[1,64,8]{1,2,0:T(8,128)} %bitcast.23), channel_id=1, replica_groups=mesh['grp'=2,'ep'=16,'tp'=1] {'ep'}, dimensions={0}, use_global_device_ids=true | all-gather | bytes 34816 | tf_op jit(solution)/shard_map/all_gather | solution.py:42
  33.4 18.4 %all-gather.1 = f32[16,64,8]{1,2,0:T(8,128)S(1)} all-gather(f32[1,64,8]{1,2,0:T(8,128)} %bitcast.24), channel_id=1, replica_groups=mesh['grp'=2,'ep'=16,'tp'=1] {'ep'}, dimensions={0}, use_global_device_ids=true | all-gather | bytes 34816 | tf_op jit(solution)/shard_map/all_gather | solution.py:43
  51.9 0.2 reduce_window_sum.14
  52.1 0.4 select_reduce_fusion.1
  52.5 0.1 broadcast_add_fusion
  52.5 0.1 add.80
  52.6 0.1 add.77
  52.7 0.2 select_reduce_fusion
  52.9 0.1 mul.59
  53.0 0.4 fusion.19
  53.3 0.1 broadcast_in_dim.66
  53.5 9.7 %all-gather.4.cloned.1.call-done = bf16[1024,2048]{1,0:T(8,128)(2,1)} async-done(((bf16[64,2048]{1,0:T(8,128)(2,1)}), bf16[1024,2048]{1,0:T(8,128)(2,1)}) %all-gather.4.cloned.1.call-update) | async-done | bytes 4194320 | tf_op jit(solution)/shard_map/all_gather | solution.py:41
  63.2 11.7 %gather_fusion = bf16[1024,2048]{1,0:T(8,128)(2,1)} fusion(bf16[1024,2048]{1,0:T(8,128)(2,1)} %all-gather.4.cloned.1.call-done, s32[1024]{0:T(1024)S(1)} %broadcast_clamp_fusion), kind=kCustom, calls=%fused_computation | custom fusion | bytes 8392704 | tf_op jit(solution)/shard_map/jit(_take)/gather | solution.py:62
  75.0 6.6 %fusion.6 = f32[1024,512]{1,0:T(8,128)} fusion(bf16[1,2048,512]{2,1,0:T(8,128)(2,1)} %param.13, bf16[1024,2048]{1,0:T(8,128)(2,1)} %gather_fusion, pred[1024]{0:T(1024)(128)(4,1)S(1)} %compare_and_fusion, pred[1024]{0:T(1024)(128)(4,1)S(1)} %broadcast_in_dim.66), kind=kOutput, calls=%fused_computation.11 | convolution fusion | flops 2151677952 | bytes 8390656 | tf_op jit(solution)/shard_map/dot_general | solution.py:15
  81.5 0.0 copy-done
  81.5 9.2 %convolution_convert_fusion = bf16[1024,2048]{1,0:T(8,128)(2,1)} fusion(bf16[1,512,2048]{2,1,0:T(8,128)(2,1)S(1)} %copy-done, f32[1024,512]{1,0:T(8,128)} %fusion.6, bf16[1,2048,512]{2,1,0:T(8,128)(2,1)} %param.12, bf16[1024,2048]{1,0:T(8,128)(2,1)} %gather_fusion, pred[1024]{0:T(1024)(128)(4,1)S(1)} %compare_and_fusion, ...), kind=kOutput, calls=%fused_computation.8 | convolution fusion | flops 4304404480 | bytes 14682112 | tf_op jit(solution)/shard_map/dot_general | solution.py:17
  90.7 18.6 %scatter_custom_fusion = f32[1024,2048]{1,0:T(8,128)} fusion(s32[1024]{0:T(1024)S(1)} %bitcast.22, bf16[1024,2048]{1,0:T(8,128)(2,1)} %convolution_convert_fusion, f32[1024]{0:T(1024)S(1)} %mul.59, f32[]{:T(128)} %constant.13.clone.1), kind=kCustom, calls=%fused_computation.2 | custom fusion | flops 6291456 | bytes 12587012 | tf_op jit(solution)/shard_map/scatter-add | solution.py:77
  109.3 0.0 copy-start.1
  109.3 0.0 reduce-scatter.2.cloned.1.call-update
  109.4 0.9 copy-done.1
  110.3 2.1 fusion.28
  112.4 3.5 %convolution_convert_fusion.1 = bf16[64,2048]{1,0:T(8,128)(2,1)S(1)} fusion(bf16[512,2048]{1,0:T(8,128)(2,1)} %param.17, bf16[64,2048]{1,0:T(8,128)(2,1)S(1)} %copy-done.1, bf16[2048,512]{1,0:T(8,128)(2,1)} %param.16, f32[64,512]{1,0:T(8,128)S(1)} %fusion.28), kind=kOutput, calls=%fused_computation.9 | convolution fusion | flops 268763136 | bytes 4849664 | tf_op jit(solution)/shard_map/dot_general | solution.py:17
  115.9 95.8 %reduce-scatter.2.cloned.1.call-done = f32[64,2048]{1,0:T(8,128)} async-done(((f32[1024,2048]{1,0:T(8,128)}), f32[64,2048]{1,0:T(8,128)}) %reduce-scatter.2.cloned.1.call-update) | async-done | bytes 524304 | tf_op jit(solution)/shard_map/reduce_scatter | solution.py:79
  211.6 1.8 add_convert_fusion
  (9 shorter events, 0.1 us)
Async XLA Ops:
  6.5 75.0 %copy-start = (bf16[1,512,2048]{2,1,0:T(8,128)(2,1)S(1)}, bf16[1,512,2048]{2,1,0:T(8,128)(2,1)}, u32[]{:S(2)}) copy-start(bf16[1,512,2048]{2,1,0:T(8,128)(2,1)} %param.14) | copy-start | bytes 6291460
  6.5 56.7 %all-gather.4.cloned.1.call-start = ((), (), s32[]{:S(2)}) async-start(), calls=%async_computation.1 | async-start | bytes 4456448 | tf_op jit(solution)/shard_map/all_gather | solution.py:41
  9.6 202.0 %reduce-scatter.2.cloned.1.call-start = ((), (), s32[]{:S(2)}) async-start(), calls=%async_computation.2 | async-start | bytes 8912896 | tf_op jit(solution)/shard_map/reduce_scatter | solution.py:79
  109.3 0.9 copy-start.1
Sparse Core Ops, SparseCore 0:
  9.7 53.4 all-gather.3
  109.5 102.0 reduce-scatter.1
where the time goes:
time: 221 us; the launch traced here: 220 us
  waiting for transfers between devices  106 us (48%)
  blocking collectives  42.1 us (19%)
  other arithmetic  24.8 us (11%)
  matrix products  21.3 us (10%)
  between operations  13.5 us (6%)
  local copies, waits for them, and re-layouts  13 us (6%)
    reduce_scatter x1, waiting for transfers between devices, per_device(): routed = lax.psum_scatter(terms, 'ep', scatter_dimension=0, tiled=True)  95.8 us
    all_gather x1, blocking collectives, per_device(): all_routes = lax.all_gather(routes, 'ep', axis=0, tiled=True)  23.8 us
    scatter-add x1, other arithmetic, per_device(): jnp.zeros((experts * tok_rows, half_width), jnp.float32).at[global_row]  18.6 us
    all_gather x1, blocking collectives, per_device(): all_weights = lax.all_gather(route_weights, 'ep', axis=0, tiled=True)  18.4 us
    dot_general x2, matrix products, swiglu_partial(): partial_value = jnp.dot(hidden, w_down, preferred_element_type=jnp.float32)  12.7 us
    gather x1, local copies, waits for them, and re-layouts, per_device(): taken = jnp.take(all_normed, global_row, axis=0)  11.7 us
    all_gather x1, waiting for transfers between devices, per_device(): all_normed = lax.all_gather(normed, 'ep', axis=0, tiled=True)  9.75 us
    dot_general x1, matrix products, swiglu_partial(): up_proj = jnp.dot(row_block, w_up, preferred_element_type=jnp.float32)  6.57 us
  transfers between devices with their start and end apart: 2, of which 2 were waited for; matrix products, arithmetic and copies ran while one was open for 3% of the time, Pallas kernels for 0%

commit v1 on v0

--- a/solution.py
+++ b/solution.py
@@ -2,6 +2,16 @@
 import jax.numpy as jnp
 from jax import lax
 from jax.sharding import PartitionSpec as P
+
+
+def cut_axis_part_for(local_array, local_values):
+    return jnp.split(
+        lax.all_gather(
+            jnp.concatenate([local_array, local_values], axis=1), axis_name="ep", axis=0, tiled=True
+        ),
+        [local_array.shape[1]],
+        axis=1,
+    )
 
 
 def rms_scaled(values, gain):
@@ -39,8 +49,7 @@
     normed = rms_scaled(tokens, norm_gain)
     shared_part = swiglu_partial(normed, shared_gate, shared_up, shared_down)
     all_normed = lax.all_gather(normed, "ep", axis=0, tiled=True)
-    all_routes = lax.all_gather(routes, "ep", axis=0, tiled=True)
-    all_weights = lax.all_gather(route_weights, "ep", axis=0, tiled=True)
+    all_routes, all_weights = cut_axis_part_for(routes, route_weights)
     own_expert = lax.axis_index("ep")
     hit_table = all_routes == own_expert
     is_mine = jnp.sum(hit_table.astype(jnp.int32), axis=1).reshape(experts, tok_rows)

time: 221 us -> 220 us (level)
  blocking collectives: 42.1 us -> 23.7 us
  waiting for transfers between devices: 106 us -> 122 us
    all_gather x2 -> x1, blocking collectives: 42.1 us -> 23.7 us  [cut_axis_part_for(): lax.all_gather(jnp.concatenate([local_array, local_values], axis=1), axis...]
    all_gather x1, waiting for transfers between devices: 9.75 us -> 26.2 us  [per_device(): all_normed = lax.all_gather(normed, 'ep', axis=0, tiled=True)]
  transfers between devices with their start and end apart: 2 -> 2, of which waited for: 2 -> 2; matrix products, arithmetic and copies ran while one was open for 3% -> 4% of each run, Pallas kernels for 0% -> 0%
where the time goes in v1:
time: 220 us
  waiting for transfers between devices  122 us (55%)
  other arithmetic  26.1 us (12%)
  blocking collectives  23.7 us (11%)
  matrix products  21.3 us (10%)
  between operations  13.5 us (6%)
  local copies, waits for them, and re-layouts  13.3 us (6%)
    reduce_scatter x1, waiting for transfers between devices, per_device(): routed = lax.psum_scatter(terms, 'ep', scatter_dimension=0, tiled=True)  95.6 us
    all_gather x1, waiting for transfers between devices, per_device(): all_normed = lax.all_gather(normed, 'ep', axis=0, tiled=True)  26.2 us
    all_gather x1, blocking collectives, cut_axis_part_for(): lax.all_gather(jnp.concatenate([local_array, local_values], axis=1), axis...  23.7 us
    scatter-add x1, other arithmetic, per_device(): jnp.zeros((experts * tok_rows, half_width), jnp.float32).at[global_row]  18.6 us
    dot_general x2, matrix products, swiglu_partial(): partial_value = jnp.dot(hidden, w_down, preferred_element_type=jnp.float32)  12.7 us
    gather x1, local copies, waits for them, and re-layouts, per_device(): taken = jnp.take(all_normed, global_row, axis=0)  11.7 us
    dot_general x1, matrix products, swiglu_partial(): up_proj = jnp.dot(row_block, w_up, preferred_element_type=jnp.float32)  6.58 us
  transfers between devices with their start and end apart: 2, of which 2 were waited for; matrix products, arithmetic and copies ran while one was open for 4% of the time, Pallas kernels for 0%

profile of v1, /device:TPU:0, one launch (start us, length us, event | category | flops | bytes accessed | tf_op | source)
XLA Modules:
  0.0 219.9 jit_solution(17964895184227281096)
XLA Ops:
  6.5 0.0 copy-start
  6.5 0.0 all-gather.3.cloned.1.call-start
  6.5 1.2 fusion.15
  7.8 1.8 fusion.17
  9.6 0.0 all-gather.3.cloned.1.call-update
  9.6 0.0 reduce-scatter.2.cloned.1.call-start
  9.7 0.7 convert_element_type.44
  10.4 0.7 maximum_bitcast_fusion
  11.1 23.7 %all-gather = f32[16,64,16]{1,2,0:T(8,128)S(1)} all-gather(f32[1,64,16]{1,2,0:T(8,128)S(1)} %maximum_bitcast_fusion), channel_id=1, replica_groups=mesh['grp'=2,'ep'=16,'tp'=1] {'ep'}, dimensions={0}, use_global_device_ids=true | all-gather | bytes 69632 | tf_op jit(solution)/shard_map/all_gather | solution.py:9
  34.8 0.1 reshape.93
  35.0 0.1 reduce_window_sum.13
  35.0 0.2 reduce_window_sum.14
  35.3 0.4 select_reduce_fusion.1
  35.6 0.1 broadcast_add_fusion
  35.7 0.1 add.80
  35.8 0.1 add.77
  35.9 0.1 broadcast_in_dim.72
  35.9 0.2 select_reduce_fusion
  36.2 0.1 mul.59
  36.2 0.4 fusion.19
  36.6 0.1 broadcast_in_dim.66
  36.7 26.2 %all-gather.3.cloned.1.call-done = bf16[1024,2048]{1,0:T(8,128)(2,1)} async-done(((bf16[64,2048]{1,0:T(8,128)(2,1)}), bf16[1024,2048]{1,0:T(8,128)(2,1)}) %all-gather.3.cloned.1.call-update) | async-done | bytes 4194320 | tf_op jit(solution)/shard_map/all_gather | solution.py:51
  63.0 11.7 %gather_fusion = bf16[1024,2048]{1,0:T(8,128)(2,1)} fusion(bf16[1024,2048]{1,0:T(8,128)(2,1)} %all-gather.3.cloned.1.call-done, s32[1024]{0:T(1024)S(1)} %broadcast_clamp_fusion), kind=kCustom, calls=%fused_computation | custom fusion | bytes 8392704 | tf_op jit(solution)/shard_map/jit(_take)/gather | solution.py:71
  74.7 6.6 %fusion.6 = f32[1024,512]{1,0:T(8,128)} fusion(bf16[1,2048,512]{2,1,0:T(8,128)(2,1)} %param.13, bf16[1024,2048]{1,0:T(8,128)(2,1)} %gather_fusion, pred[1024]{0:T(1024)(128)(4,1)S(1)} %compare_and_fusion, pred[1024]{0:T(1024)(128)(4,1)S(1)} %broadcast_in_dim.66), kind=kOutput, calls=%fused_computation.11 | convolution fusion | flops 2151677952 | bytes 8390656 | tf_op jit(solution)/shard_map/dot_general | solution.py:25
  81.3 0.0 copy-done
  81.3 9.2 %convolution_convert_fusion = bf16[1024,2048]{1,0:T(8,128)(2,1)} fusion(bf16[1,512,2048]{2,1,0:T(8,128)(2,1)S(1)} %copy-done, f32[1024,512]{1,0:T(8,128)} %fusion.6, bf16[1,2048,512]{2,1,0:T(8,128)(2,1)} %param.12, bf16[1024,2048]{1,0:T(8,128)(2,1)} %gather_fusion, pred[1024]{0:T(1024)(128)(4,1)S(1)} %compare_and_fusion, ...), kind=kOutput, calls=%fused_computation.8 | convolution fusion | flops 4304404480 | bytes 14682112 | tf_op jit(solution)/shard_map/dot_general | solution.py:27
  90.5 18.6 %scatter_custom_fusion = f32[1024,2048]{1,0:T(8,128)} fusion(s32[1024]{0:T(1024)S(1)} %bitcast.24, bf16[1024,2048]{1,0:T(8,128)(2,1)} %convolution_convert_fusion, f32[1024]{0:T(1024)S(1)} %mul.59, f32[]{:T(128)} %constant.13.clone.1), kind=kCustom, calls=%fused_computation.2 | custom fusion | flops 6291456 | bytes 12587012 | tf_op jit(solution)/shard_map/scatter-add | solution.py:86
  109.1 0.0 copy-start.1
  109.1 0.0 reduce-scatter.2.cloned.1.call-update
  109.1 0.9 copy-done.1
  110.0 2.1 fusion.29
  112.1 3.5 %convolution_convert_fusion.1 = bf16[64,2048]{1,0:T(8,128)(2,1)S(1)} fusion(bf16[512,2048]{1,0:T(8,128)(2,1)} %param.17, bf16[64,2048]{1,0:T(8,128)(2,1)S(1)} %copy-done.1, bf16[2048,512]{1,0:T(8,128)(2,1)} %param.16, f32[64,512]{1,0:T(8,128)S(1)} %fusion.29), kind=kOutput, calls=%fused_computation.9 | convolution fusion | flops 268763136 | bytes 4849664 | tf_op jit(solution)/shard_map/dot_general | solution.py:27
  115.6 95.6 %reduce-scatter.2.cloned.1.call-done = f32[64,2048]{1,0:T(8,128)} async-done(((f32[1024,2048]{1,0:T(8,128)}), f32[64,2048]{1,0:T(8,128)}) %reduce-scatter.2.cloned.1.call-update) | async-done | bytes 524304 | tf_op jit(solution)/shard_map/reduce_scatter | solution.py:88
  211.2 1.8 add_convert_fusion
  (10 shorter events, 0.1 us)
Async XLA Ops:
  6.5 74.7 %copy-start = (bf16[1,512,2048]{2,1,0:T(8,128)(2,1)S(1)}, bf16[1,512,2048]{2,1,0:T(8,128)(2,1)}, u32[]{:S(2)}) copy-start(bf16[1,512,2048]{2,1,0:T(8,128)(2,1)} %param.14) | copy-start | bytes 6291460
  6.5 56.4 %all-gather.3.cloned.1.call-start = ((), (), s32[]{:S(2)}) async-start(), calls=%async_computation.1 | async-start | bytes 4456448 | tf_op jit(solution)/shard_map/all_gather | solution.py:51
  9.6 201.6 %reduce-scatter.2.cloned.1.call-start = ((), (), s32[]{:S(2)}) async-start(), calls=%async_computation.2 | async-start | bytes 8912896 | tf_op jit(solution)/shard_map/reduce_scatter | solution.py:88
  109.1 0.9 copy-start.1
Sparse Core Ops, SparseCore 0:
  9.7 53.1 all-gather.2
  109.2 101.9 reduce-scatter.1
